TPU v7x, 512 devices: a whole 4x8x8 slice. The times are simulated.
512 devices in a mesh: rep: 2 (over z_hi), fs: 32 (over z_lo, y), tp: 8 (over x, core).
Axes of the slice: x: 4, y: 8, z: 8 (z_hi: 2, z_lo: 4; z = z_hi * 4 + z_lo), core: 2. Of those that a mesh axis runs over, the one named last changes fastest.
Arguments:
- tokens: bfloat16 [20480, 2048], P(('rep', 'fs')), may hold values from -6 to 6
- gate_weight: float32 [2048, 5120], P('fs', 'tp'), may hold values from -0.125 to 0.125
- up_weight: float32 [2048, 5120], P('fs', 'tp'), may hold values from -0.125 to 0.125
- down_weight: float32 [2048, 5120], P('fs', 'tp'), may hold values from -0.078125 to 0.078125
- value_weight: float32 [2048, 2048], P('fs', 'tp'), may hold values from -0.125 to 0.125
- glu_weight: float32 [2048, 2048], P('fs', 'tp'), may hold values from -0.125 to 0.125
- out_weight: float32 [2048, 2048], P('fs', 'tp'), may hold values from -0.125 to 0.125
- gate_scale: float32 [5120], P('tp'), may hold values from 0.1 to 1.9
- up_scale: float32 [5120], P('tp'), may hold values from 0.5 to 2
- down_scale: float32 [2048], P('fs'), may hold values from 1 to 4
- value_scale: float32 [2048], P('tp'), may hold values from 0.2 to 3.4
- glu_scale: float32 [2048], P('tp'), may hold values from 0.1 to 1.9
- out_scale: float32 [2048], P('fs'), may hold values from 1 to 4
- conv_kernel: float32 [31, 2048], P(None, 'tp'), may hold values from -1 to 1
- norm_gain: float32 [2048], P('tp'), may hold values from 0.1 to 1.9
- first_gain: float32 [2048], replicated, may hold values from 0.1 to 1.9
- conv_gain: float32 [2048], replicated, may hold values from 0.1 to 1.9
- second_gain: float32 [2048], replicated, may hold values from 0.1 to 1.9
Outputs:
- result: bfloat16 [20480, 2048], P(('rep', 'fs'))
All inputs are finite; a program needn't handle non-finite values.
Results may differ from a plain program's by a relative error of at most 0.02.
Values may be sent and summed in bfloat16 or wider, within the bound.
No kernel may reach another device: no remote copies, remote signals or barrier semaphores. Data moves between devices by JAX's collectives and lax.ppermute only.
A program may use at most 64 MiB of HBM per device.

v0:
```python
import jax
import jax.numpy as jnp
from jax import lax
from jax.sharding import PartitionSpec as P

D = 2048
EPSILON = 1e-06


def split_up(shard, dim, size):
    before, after = (shard.shape[:dim], shard.shape[dim + 1 :])
    return jnp.moveaxis(shard.reshape(*before, size, -1, *after), dim, 0)


def sum_at_owner(shard, axis, dim):
    size = lax.axis_size(axis)
    parts = lax.all_to_all(split_up(shard, dim, size), axis, 0, 0, tiled=True)
    return jnp.sum(parts.astype(jnp.float32), axis=0)


def side_by_side(arrays, axis, dim, along):
    widths = [a.shape[along] for a in arrays]
    both = jnp.concatenate(arrays, axis=along)
    out = lax.all_gather(both, axis, axis=dim, tiled=True)
    return tuple(jnp.split(out, [sum(widths[:k]) for k in range(1, len(widths))], axis=along))


def rows_first(arrays, axis, dims):
    turned = [jnp.moveaxis(a, dim, 0) for a, dim in zip(arrays, dims)]
    both = jnp.concatenate([t.reshape(len(t), -1) for t in turned], axis=1)
    out, at, outs = (lax.all_gather(both, axis, axis=0, tiled=True), 0, [])
    for t, dim in zip(turned, dims):
        slab = out[:, at : at + t[0].size].reshape(-1, *t.shape[1:])
        outs.append(jnp.moveaxis(slab, 0, dim))
        at += t[0].size
    return tuple(outs)


def in_order(parts, dim):
    shape = list(parts.shape[1:])
    shape[dim] *= parts.shape[0]
    return jnp.moveaxis(parts, 0, dim).reshape(shape)


def copy_for_each(shard, axis):
    size = lax.axis_size(axis)
    return lax.all_to_all(
        jnp.broadcast_to(shard[None], (size, *shard.shape)), axis, 0, 0, tiled=True
    )


def collect(shard, axis, dim):
    return in_order(copy_for_each(shard, axis), dim)


def over_copies(shard, axis):
    return copy_for_each(shard, axis).sum(axis=0)


def in_one(arrays, axis):
    ravelled, at, outs = (jnp.concatenate([a.reshape(-1) for a in arrays]), 0, [])
    running = over_copies(ravelled, axis)
    for a in arrays:
        outs.append(running[at : at + a.size].reshape(a.shape))
        at += a.size
    return tuple(outs)


def rms_rows(rows, gains):
    values = rows.astype(jnp.float32)
    scaled = values * lax.rsqrt(jnp.mean(values * values, axis=-1, keepdims=True) + EPSILON)
    return (scaled * gains).astype(jnp.bfloat16)


def gated_hidden(normed, gate_full, up_full, gate_scale, up_scale):
    gate_part = jnp.dot(normed, gate_full, preferred_element_type=jnp.float32) * gate_scale
    upward = jnp.dot(normed, up_full, preferred_element_type=jnp.float32) * up_scale
    return (jax.nn.silu(gate_part) * upward).astype(jnp.bfloat16)


def causal_depthwise(inputs, kernel):
    taps = kernel.shape[0]
    length = inputs.shape[0]
    padded = jnp.concatenate(
        [jnp.zeros((taps - 1, inputs.shape[1]), jnp.float32), inputs.astype(jnp.float32)], axis=0
    )
    total = jnp.zeros((length, inputs.shape[1]), jnp.float32)
    for offset in range(taps):
        total = total + kernel[offset] * padded[offset : offset + length]
    return total


def branch_sum(active, weight_rows):
    return sum_at_owner(
        lax.dot_general(
            active, weight_rows, (((1,), (1,)), ((), ())), preferred_element_type=jnp.float32
        ).astype(jnp.bfloat16),
        "tp",
        0,
    )


def local(
    tokens,
    gate_weight,
    up_weight,
    down_weight,
    value_weight,
    glu_weight,
    out_weight,
    gate_scale,
    up_scale,
    down_scale,
    value_scale,
    glu_scale,
    out_scale,
    conv_kernel,
    norm_gain,
    first_gain,
    conv_gain,
    second_gain,
):
    gate_cast = gate_weight.astype(jnp.bfloat16)
    up_cast = up_weight.astype(jnp.bfloat16)
    down_cast = down_weight.astype(jnp.bfloat16)
    value_cast = value_weight.astype(jnp.bfloat16)
    glu_cast = glu_weight.astype(jnp.bfloat16)
    out_cast = out_weight.astype(jnp.bfloat16)
    gate_full, up_full, down_full, value_full, glu_full, out_full = side_by_side(
        (gate_cast, up_cast, down_cast, value_cast, glu_cast, out_cast), "fs", 0, 1
    )
    down_rows, out_rows = rows_first((down_scale, out_scale), "fs", (0, 0))
    members = lax.axis_size("tp")
    own_rows = tokens.shape[0] // members
    first_row = lax.axis_index("tp") * own_rows
    hidden = gated_hidden(rms_rows(tokens, first_gain), gate_full, up_full, gate_scale, up_scale)
    own_tokens = lax.dynamic_slice_in_dim(tokens, first_row, own_rows, 0)
    after_first = (
        own_tokens.astype(jnp.float32) + 0.5 * down_rows * branch_sum(hidden, down_full)
    ).astype(jnp.bfloat16)
    rows = collect(rms_rows(after_first, conv_gain), "tp", 0)
    value_part = jnp.dot(rows, value_full, preferred_element_type=jnp.float32) * value_scale
    gate_part = jnp.dot(rows, glu_full, preferred_element_type=jnp.float32) * glu_scale
    glu_in = (value_part * jax.nn.sigmoid(gate_part)).astype(jnp.bfloat16)
    mixed = causal_depthwise(glu_in, conv_kernel)
    row_sums, row_squares = in_one((jnp.sum(mixed, axis=1), jnp.sum(mixed * mixed, axis=1)), "tp")
    mean_rows = (row_sums / D)[:, None]
    square_rows = (row_squares / D)[:, None]
    normalized = (
        (mixed - mean_rows) * lax.rsqrt(square_rows - mean_rows * mean_rows + EPSILON) * norm_gain
    )
    active = jax.nn.silu(normalized).astype(jnp.bfloat16)
    after_conv = (after_first.astype(jnp.float32) + out_rows * branch_sum(active, out_full)).astype(
        jnp.bfloat16
    )
    hidden = gated_hidden(
        collect(rms_rows(after_conv, second_gain), "tp", 0),
        gate_full,
        up_full,
        gate_scale,
        up_scale,
    )
    after_second = (
        after_conv.astype(jnp.float32) + 0.5 * down_rows * branch_sum(hidden, down_full)
    ).astype(jnp.bfloat16)
    return collect(after_second, "tp", 0)


def solution(mesh):
    placed = (
        P(("rep", "fs"), None),
        P("fs", "tp"),
        P("fs", "tp"),
        P("fs", "tp"),
        P("fs", "tp"),
        P("fs", "tp"),
        P("fs", "tp"),
        P("tp"),
        P("tp"),
        P("fs"),
        P("tp"),
        P("tp"),
        P("fs"),
        P(None, "tp"),
        P("tp"),
        P(),
        P(),
        P(),
    )
    return jax.shard_map(
        local, mesh=mesh, in_specs=placed, out_specs=P(("rep", "fs"), None), check_vma=False
    )
```

profile of v0, /device:TPU:1, one launch (start us, length us, event | category | flops | bytes accessed | tf_op | source)
XLA Modules:
  0.0 425.5 jit_solution(13172832336793089133)
XLA Ops:
  6.5 1.0 convert_dynamic-update-slice_fusion.2
  7.6 0.9 convert_dynamic-update-slice_fusion.1
  8.5 0.9 convert_dynamic-update-slice_fusion
  9.4 0.8 convert_dynamic-update-slice_fusion.5
  10.3 0.8 convert_dynamic-update-slice_fusion.4
  11.1 0.8 convert_dynamic-update-slice_fusion.3
  12.0 0.7 copy-done.1
  12.7 1.7 fusion
  14.4 158.1 %all-gather.3.cloned.1.call-done = bf16[2048,2688]{1,0:T(8,128)(2,1)} async-done(((bf16[64,2688]{1,0:T(8,128)(2,1)}), bf16[2048,2688]{1,0:T(8,128)(2,1)}) %all-gather.3.cloned.1.call-update) | async-done | bytes 11010064 | tf_op jit(solution)/shard_map/all_gather | solution.py:24
  172.5 3.0 fusion.13
  175.5 6.3 %convolution_convert_fusion.2 = bf16[320,2048]{1,0:T(8,128)(2,1)} fusion(bf16[2048,2688]{1,0:T(8,128)(2,1)} %all-gather.3.cloned.1.call-done, f32[320,640]{1,0:T(8,128)S(1)} %fusion.13, f32[640]{0:T(1024)S(1)} %copy-done.9, bf16[320,2048]{1,0:T(8,128)(2,1)S(1)} %copy-done, f32[2048]{0:T(1024)S(1)} %copy-done.7, f32[320]{0:T(512)S(1)} %add_rsqrt_fusion.1), kind=kOutput, calls=%fused_computation.4 | convolution fusion | flops 1682432000 | bytes 8695552 | tf_op jit(solution)/shard_map/dot_general | solution.py:95
  181.8 23.9 %all-to-all-start = ((bf16[8,40,2048]{2,1,0:T(8,128)(2,1)}), bf16[8,40,2048]{2,1,0:T(8,128)(2,1)S(1)}, u32[]{:S(2)}, u32[]{:S(2)}) async-start(bf16[8,40,2048]{2,1,0:T(8,128)(2,1)} %bitcast.52), calls=%async_computation | async-start | bytes 2621440 | tf_op jit(solution)/shard_map/all_to_all | solution.py:17
  205.7 62.5 %all-gather = f32[32,64,2]{1,2,0:T(2,128)S(1)} all-gather(f32[1,64,2]{1,2,0:T(2,128)S(1)} %maximum_bitcast_fusion), channel_id=1, replica_groups=mesh['rep'=2,'fs'=32,'tp'=8] {'fs'}, dimensions={0}, use_global_device_ids=true | all-gather | bytes 16896 | tf_op jit(solution)/shard_map/all_gather | solution.py:31
  268.3 0.2 convert_reduce_fusion.2
  268.5 0.2 fusion.68
  268.8 1.2 broadcast_in_dim.8
  270.0 19.0 %all-to-all-start.1 = ((bf16[8,40,2048]{2,1,0:T(8,128)(2,1)}), bf16[8,40,2048]{2,1,0:T(8,128)(2,1)S(1)}, u32[]{:S(2)}, u32[]{:S(2)}) async-start(bf16[8,40,2048]{2,1,0:T(8,128)(2,1)} %broadcast_in_dim.8), calls=%async_computation.1 | async-start | bytes 2621440 | tf_op jit(solution)/shard_map/all_to_all | solution.py:47
  289.1 17.7 %all-to-all-done.1 = bf16[8,40,2048]{2,1,0:T(8,128)(2,1)S(1)} async-done(((bf16[8,40,2048]{2,1,0:T(8,128)(2,1)}), bf16[8,40,2048]{2,1,0:T(8,128)(2,1)S(1)}, u32[]{:S(2)}, u32[]{:S(2)}) %all-to-all-start.1) | async-done | bytes 1310752 | tf_op jit(solution)/shard_map/all_to_all | solution.py:47
  306.8 1.8 fusion.40
  308.6 1.8 fusion.43
  310.4 1.3 fusion.138
  311.8 8.0 %all_to_all.36 = f32[8,1,640]{2,1,0:T(1,128)S(1)} all-to-all(f32[8,1,640]{2,1,0:T(1,128)S(1)} %broadcast_in_dim.9), channel_id=1, replica_groups=mesh['rep'=2,'fs'=32,'tp'=8] {'tp'}, dimensions={0} | all-to-all | bytes 40960 | tf_op jit(solution)/shard_map/all_to_all | solution.py:47
  319.9 1.8 convolution_convert_fusion.1
  321.8 20.9 %all_to_all.37 = bf16[8,40,2048]{2,1,0:T(8,128)(2,1)S(1)} all-to-all(bf16[8,40,2048]{2,1,0:T(8,128)(2,1)S(1)} %bitcast.53), channel_id=1, replica_groups=mesh['rep'=2,'fs'=32,'tp'=8] {'tp'}, dimensions={0} | all-to-all | bytes 2621440 | tf_op jit(solution)/shard_map/all_to_all | solution.py:17
  342.6 0.2 convert_reduce_fusion.1
  343.3 21.2 %all_to_all.38 = bf16[8,40,2048]{2,1,0:T(8,128)(2,1)S(1)} all-to-all(bf16[8,40,2048]{2,1,0:T(8,128)(2,1)S(1)} %broadcast_in_dim.10), channel_id=1, replica_groups=mesh['rep'=2,'fs'=32,'tp'=8] {'tp'}, dimensions={0} | all-to-all | bytes 2621440 | tf_op jit(solution)/shard_map/all_to_all | solution.py:47
  364.5 2.9 fusion.16
  367.4 6.3 %convolution_convert_fusion = bf16[320,2048]{1,0:T(8,128)(2,1)} fusion(bf16[2048,2688]{1,0:T(8,128)(2,1)} %all-gather.3.cloned.1.call-done, bf16[320,2048]{1,0:T(8,128)(2,1)S(1)} %bitcast.55, f32[320,640]{1,0:T(8,128)S(1)} %fusion.16, f32[640]{0:T(1024)S(1)} %copy-done.9), kind=kOutput, calls=%fused_computation.2 | convolution fusion | flops 1679810560 | bytes 8686080 | tf_op jit(solution)/shard_map/dot_general | solution.py:95
  373.8 22.3 %all_to_all.39 = bf16[8,40,2048]{2,1,0:T(8,128)(2,1)S(1)} all-to-all(bf16[8,40,2048]{2,1,0:T(8,128)(2,1)} %bitcast.56), channel_id=1, replica_groups=mesh['rep'=2,'fs'=32,'tp'=8] {'tp'}, dimensions={0} | all-to-all | bytes 2621440 | tf_op jit(solution)/shard_map/all_to_all | solution.py:17
  396.0 0.2 convert_reduce_fusion
  396.4 21.2 %all_to_all.40 = bf16[8,40,2048]{2,1,0:T(8,128)(2,1)S(1)} all-to-all(bf16[8,40,2048]{2,1,0:T(8,128)(2,1)S(1)} %broadcast_in_dim.11), channel_id=1, replica_groups=mesh['rep'=2,'fs'=32,'tp'=8] {'tp'}, dimensions={0} | all-to-all | bytes 2621440 | tf_op jit(solution)/shard_map/all_to_all | solution.py:47
  417.6 1.1 copy.33
  (47 shorter events, 1.2 us)
Async XLA Ops:
  6.5 166.0 %copy-start = (bf16[320,2048]{1,0:T(8,128)(2,1)S(1)}, bf16[320,2048]{1,0:T(8,128)(2,1)}, u32[]{:S(2)}) copy-start(bf16[320,2048]{1,0:T(8,128)(2,1)} %param.18) | copy-start | bytes 3932164
  6.5 166.0 %copy-start.7 = (f32[2048]{0:T(1024)S(1)}, f32[2048]{0:T(1024)}, u32[]{:S(2)}) copy-start(f32[2048]{0:T(1024)} %param.33) | copy-start | bytes 24580
  6.5 166.0 %copy-start.8 = (f32[640]{0:T(1024)S(1)}, f32[640]{0:T(1024)}, u32[]{:S(2)}) copy-start(f32[640]{0:T(1024)} %param.25) | copy-start | bytes 7684
  6.5 165.9 %all-gather.3.cloned.1.call-start = ((), (), s32[]{:S(2)}) async-start(), calls=%async_computation.7 | async-start | bytes 11354112 | tf_op jit(solution)/shard_map/all_gather | solution.py:24
  12.0 0.7 copy-start.1
  14.4 161.1 %copy-start.9 = (f32[640]{0:T(1024)S(1)}, f32[640]{0:T(1024)}, u32[]{:S(2)}) copy-start(f32[640]{0:T(1024)} %param.26) | copy-start | bytes 7684
  181.8 23.9 %copy-start.5 = (f32[64]{0:T(128)S(1)}, f32[64]{0:T(128)}, u32[]{:S(2)}) copy-start(f32[64]{0:T(128)} %param.30) | copy-start | bytes 772
  181.8 23.9 %copy-start.6 = (f32[64]{0:T(128)S(1)}, f32[64]{0:T(128)}, u32[]{:S(2)}) copy-start(f32[64]{0:T(128)} %param.27) | copy-start | bytes 772
  181.8 86.9 %copy-start.3 = (f32[2048]{0:T(1024)S(1)}, f32[2048]{0:T(1024)}, u32[]{:S(2)}) copy-start(f32[2048]{0:T(1024)} %param.34) | copy-start | bytes 24580
  181.8 86.5 %all-to-all-start = ((bf16[8,40,2048]{2,1,0:T(8,128)(2,1)}), bf16[8,40,2048]{2,1,0:T(8,128)(2,1)S(1)}, u32[]{:S(2)}, u32[]{:S(2)}) async-start(bf16[8,40,2048]{2,1,0:T(8,128)(2,1)} %bitcast.52), calls=%async_computation | async-start | bytes 2621440 | tf_op jit(solution)/shard_map/all_to_all | solution.py:17
  268.5 20.5 %copy-start.2 = (f32[31,256]{1,0:T(8,128)S(1)}, f32[31,256]{1,0:T(8,128)}, u32[]{:S(2)}) copy-start(f32[31,256]{1,0:T(8,128)} %param.31) | copy-start | bytes 95236
  268.5 38.3 %copy-start.10 = (f32[256]{0:T(256)S(1)}, f32[256]{0:T(256)}, u32[]{:S(2)}) copy-start(f32[256]{0:T(256)} %param.29) | copy-start | bytes 3076
  270.0 36.8 %all-to-all-start.1 = ((bf16[8,40,2048]{2,1,0:T(8,128)(2,1)}), bf16[8,40,2048]{2,1,0:T(8,128)(2,1)S(1)}, u32[]{:S(2)}, u32[]{:S(2)}) async-start(bf16[8,40,2048]{2,1,0:T(8,128)(2,1)} %broadcast_in_dim.8), calls=%async_computation.1 | async-start | bytes 2621440 | tf_op jit(solution)/shard_map/all_to_all | solution.py:47
  306.8 1.8 copy-start.11
  308.6 11.3 %copy-start.12 = (f32[256]{0:T(256)S(1)}, f32[256]{0:T(256)}, u32[]{:S(2)}) copy-start(f32[256]{0:T(256)} %param.32) | copy-start | bytes 3076
  321.7 21.3 %copy-start.4 = (f32[2048]{0:T(1024)S(1)}, f32[2048]{0:T(1024)}, u32[]{:S(2)}) copy-start(f32[2048]{0:T(1024)} %param.35) | copy-start | bytes 24580
Sparse Core Ops, SparseCore 0:
  12.9 159.5 all-gather.2
where the time goes:
time: 426 us
  waiting for transfers between devices  176 us (41%)
  blocking collectives  156 us (37%)
  starting transfers between devices  42.9 us (10%)
  matrix products  23.9 us (6%)
  between operations  13.6 us (3%)
  other arithmetic  9.87 us (2%)
    all_gather x1, waiting for transfers between devices, side_by_side(): out = lax.all_gather(both, axis, axis=dim, tiled=True)  158 us
    all_gather x1, blocking collectives, rows_first(): out, at, outs = (lax.all_gather(both, axis, axis=0, tiled=True), 0, [])  62.5 us
    all_to_all x3, blocking collectives, copy_for_each(): lax.all_to_all(jnp.broadcast_to(shard[None], (size, *shard.shape)), axis,...  50.4 us
    all_to_all x2, blocking collectives, sum_at_owner(): parts = lax.all_to_all(split_up(shard, dim, size), axis, 0, 0, tiled=True)  43.1 us
    all_to_all x1, starting transfers between devices, sum_at_owner(): parts = lax.all_to_all(split_up(shard, dim, size), axis, 0, 0, tiled=True)  23.9 us
    all_to_all x1, starting transfers between devices, copy_for_each(): lax.all_to_all(jnp.broadcast_to(shard[None], (size, *shard.shape)), axis,...  19 us
    all_to_all x1, waiting for transfers between devices, copy_for_each(): lax.all_to_all(jnp.broadcast_to(shard[None], (size, *shard.shape)), axis,...  17.7 us
    dot_general x3, matrix products, branch_sum(): lax.dot_general(active, weight_rows, (((1,), (1,)), ((), ())), preferred_...  14.5 us
  transfers between devices with their start and end apart: 3, of which 2 were waited for; matrix products, arithmetic and copies ran while one was open for 0% of the time, Pallas kernels for 0%

commit v1 on v0

--- a/solution.py
+++ b/solution.py
@@ -5,6 +5,13 @@
 
 D = 2048
 EPSILON = 1e-06
+
+
+def swapped_in(x, mesh_axis, dim):
+    size = lax.axis_size(mesh_axis)
+    blocks = jnp.stack([x for _ in range(size)])
+    blocks = lax.all_to_all(blocks, mesh_axis, split_axis=0, concat_axis=0)
+    return jnp.concatenate(blocks, axis=dim)
 
 
 def split_up(shard, dim, size):
@@ -28,7 +35,7 @@
 def rows_first(arrays, axis, dims):
     turned = [jnp.moveaxis(a, dim, 0) for a, dim in zip(arrays, dims)]
     both = jnp.concatenate([t.reshape(len(t), -1) for t in turned], axis=1)
-    out, at, outs = (lax.all_gather(both, axis, axis=0, tiled=True), 0, [])
+    out, at, outs = (swapped_in(both, axis, 0), 0, [])
     for t, dim in zip(turned, dims):
         slab = out[:, at : at + t[0].size].reshape(-1, *t.shape[1:])
         outs.append(jnp.moveaxis(slab, 0, dim))

time: 426 us -> 366 us (0.86)
  blocking collectives: 156 us -> 92.5 us
    all_gather x1 -> x0, blocking collectives: 62.5 us -> none  [rows_first(): out, at, outs = (lax.all_gather(both, axis, axis=0, tiled=True), 0, [])]
    all_to_all x1, waiting for transfers between devices: 0.01 us -> 16.5 us  [sum_at_owner(): parts = lax.all_to_all(split_up(shard, dim, size), axis, 0, 0, tiled=True)]
    all_gather x1, waiting for transfers between devices: 158 us -> 143 us  [side_by_side(): out = lax.all_gather(both, axis, axis=dim, tiled=True)]
    all_to_all x1, starting transfers between devices: 19 us -> 4.44 us  [copy_for_each(): lax.all_to_all(jnp.broadcast_to(shard[None], (size, *shard.shape)), axis,...]
    all_to_all x0 -> x1, starting transfers between devices: none -> 13.5 us  [swapped_in(): blocks = lax.all_to_all(blocks, mesh_axis, split_axis=0, concat_axis=0)]
  transfers between devices with their start and end apart: 3 -> 4, of which waited for: 2 -> 3; matrix products, arithmetic and copies ran while one was open for 0% -> 4% of each run, Pallas kernels for 0% -> 0%
where the time goes in v1:
time: 366 us; the launch traced here: 365 us
  waiting for transfers between devices  177 us (48%)
  blocking collectives  92.5 us (25%)
  starting transfers between devices  41.7 us (11%)
  matrix products  23.8 us (7%)
  between operations  13.6 us (4%)
  other arithmetic  11.1 us (3%)
  local copies, waits for them, and re-layouts  4.73 us (1%)
    all_gather x1, waiting for transfers between devices, side_by_side(): out = lax.all_gather(both, axis, axis=dim, tiled=True)  143 us
    all_to_all x3, blocking collectives, copy_for_each(): lax.all_to_all(jnp.broadcast_to(shard[None], (size, *shard.shape)), axis,...  50.4 us
    all_to_all x2, blocking collectives, sum_at_owner(): parts = lax.all_to_all(split_up(shard, dim, size), axis, 0, 0, tiled=True)  42.1 us
    all_to_all x1, starting transfers between devices, sum_at_owner(): parts = lax.all_to_all(split_up(shard, dim, size), axis, 0, 0, tiled=True)  23.8 us
    all_to_all x1, waiting for transfers between devices, copy_for_each(): lax.all_to_all(jnp.broadcast_to(shard[None], (size, *shard.shape)), axis,...  17.8 us
    all_to_all x1, waiting for transfers between devices, sum_at_owner(): parts = lax.all_to_all(split_up(shard, dim, size), axis, 0, 0, tiled=True)  16.5 us
    dot_general x3, matrix products, branch_sum(): lax.dot_general(active, weight_rows, (((1,), (1,)), ((), ())), preferred_...  13.5 us
    all_to_all x1, starting transfers between devices, swapped_in(): blocks = lax.all_to_all(blocks, mesh_axis, split_axis=0, concat_axis=0)  13.5 us
  transfers between devices with their start and end apart: 4, of which 3 were waited for; matrix products, arithmetic and copies ran while one was open for 4% of the time, Pallas kernels for 0%

profile of v1, /device:TPU:1, one launch (start us, length us, event | category | flops | bytes accessed | tf_op | source)
XLA Modules:
  0.0 365.0 jit_solution(1340345547208891409)
XLA Ops:
  6.5 1.0 convert_dynamic-update-slice_fusion.2
  7.6 0.9 convert_dynamic-update-slice_fusion.1
  8.5 0.9 convert_dynamic-update-slice_fusion
  9.4 0.8 convert_dynamic-update-slice_fusion.5
  10.3 0.8 convert_dynamic-update-slice_fusion.4
  11.1 0.8 convert_dynamic-update-slice_fusion.3
  12.0 0.7 copy-done.1
  12.7 0.7 pad_maximum_fusion.1
  13.4 0.7 reshape.94
  14.1 13.5 %all-to-all-start = ((f32[32,1,128]{2,1,0:T(1,128)}), f32[32,1,128]{2,1,0:T(1,128)S(1)}, u32[]{:S(2)}, u32[]{:S(2)}) async-start(f32[32,1,128]{2,1,0:T(1,128)} %reshape.94), calls=%async_computation | async-start | bytes 32768 | tf_op jit(solution)/shard_map/all_to_all | solution.py:13
  27.6 1.7 fusion
  29.3 143.2 %all-gather.2.cloned.1.call-done = bf16[2048,2688]{1,0:T(8,128)(2,1)} async-done(((bf16[64,2688]{1,0:T(8,128)(2,1)}), bf16[2048,2688]{1,0:T(8,128)(2,1)}) %all-gather.2.cloned.1.call-update) | async-done | bytes 11010064 | tf_op jit(solution)/shard_map/all_gather | solution.py:31
  172.5 3.0 fusion.13
  175.5 6.3 %convolution_convert_fusion.2 = bf16[320,2048]{1,0:T(8,128)(2,1)} fusion(bf16[2048,2688]{1,0:T(8,128)(2,1)} %all-gather.2.cloned.1.call-done, f32[320,640]{1,0:T(8,128)S(1)} %fusion.13, f32[640]{0:T(1024)S(1)} %copy-done.7, bf16[320,2048]{1,0:T(8,128)(2,1)S(1)} %copy-done, f32[2048]{0:T(1024)S(1)} %copy-done.5, f32[320]{0:T(512)S(1)} %add_rsqrt_fusion.1), kind=kOutput, calls=%fused_computation.4 | convolution fusion | flops 1682432000 | bytes 8695552 | tf_op jit(solution)/shard_map/dot_general | solution.py:102
  181.8 23.8 %all-to-all-start.1 = ((bf16[8,40,2048]{2,1,0:T(8,128)(2,1)}), bf16[8,40,2048]{2,1,0:T(8,128)(2,1)S(1)}, u32[]{:S(2)}, u32[]{:S(2)}) async-start(bf16[8,40,2048]{2,1,0:T(8,128)(2,1)} %bitcast.51), calls=%async_computation.1 | async-start | bytes 2621440 | tf_op jit(solution)/shard_map/all_to_all | solution.py:24
  206.1 0.6 reduce.1
  206.9 16.5 %all-to-all-done.1 = bf16[8,40,2048]{2,1,0:T(8,128)(2,1)S(1)} async-done(((bf16[8,40,2048]{2,1,0:T(8,128)(2,1)}), bf16[8,40,2048]{2,1,0:T(8,128)(2,1)S(1)}, u32[]{:S(2)}, u32[]{:S(2)}) %all-to-all-start.1) | async-done | bytes 1310752 | tf_op jit(solution)/shard_map/all_to_all | solution.py:24
  223.9 1.2 broadcast_in_dim.8
  225.1 4.4 %all-to-all-start.2 = ((bf16[8,40,2048]{2,1,0:T(8,128)(2,1)}), bf16[8,40,2048]{2,1,0:T(8,128)(2,1)S(1)}, u32[]{:S(2)}, u32[]{:S(2)}) async-start(bf16[8,40,2048]{2,1,0:T(8,128)(2,1)} %broadcast_in_dim.8), calls=%async_computation.2 | async-start | bytes 2621440 | tf_op jit(solution)/shard_map/all_to_all | solution.py:54
  229.6 17.8 %all-to-all-done.2 = bf16[8,40,2048]{2,1,0:T(8,128)(2,1)S(1)} async-done(((bf16[8,40,2048]{2,1,0:T(8,128)(2,1)}), bf16[8,40,2048]{2,1,0:T(8,128)(2,1)S(1)}, u32[]{:S(2)}, u32[]{:S(2)}) %all-to-all-start.2) | async-done | bytes 1310752 | tf_op jit(solution)/shard_map/all_to_all | solution.py:54
  247.4 1.8 fusion.40
  249.2 1.7 fusion.43
  250.9 1.3 fusion.138
  252.4 8.0 %all_to_all.41 = f32[8,1,640]{2,1,0:T(1,128)S(1)} all-to-all(f32[8,1,640]{2,1,0:T(1,128)S(1)} %broadcast_in_dim.9), channel_id=1, replica_groups=mesh['rep'=2,'fs'=32,'tp'=8] {'tp'}, dimensions={0} | all-to-all | bytes 40960 | tf_op jit(solution)/shard_map/all_to_all | solution.py:54
  260.5 1.8 convolution_convert_fusion.1
  262.3 20.9 %all_to_all.42 = bf16[8,40,2048]{2,1,0:T(8,128)(2,1)S(1)} all-to-all(bf16[8,40,2048]{2,1,0:T(8,128)(2,1)S(1)} %bitcast.54), channel_id=1, replica_groups=mesh['rep'=2,'fs'=32,'tp'=8] {'tp'}, dimensions={0} | all-to-all | bytes 2621440 | tf_op jit(solution)/shard_map/all_to_all | solution.py:24
  283.8 21.2 %all_to_all.43 = bf16[8,40,2048]{2,1,0:T(8,128)(2,1)S(1)} all-to-all(bf16[8,40,2048]{2,1,0:T(8,128)(2,1)S(1)} %broadcast_in_dim.10), channel_id=1, replica_groups=mesh['rep'=2,'fs'=32,'tp'=8] {'tp'}, dimensions={0} | all-to-all | bytes 2621440 | tf_op jit(solution)/shard_map/all_to_all | solution.py:54
  305.1 3.8 %fusion.16 = f32[320,640]{1,0:T(8,128)} fusion(bf16[320,2048]{1,0:T(8,128)(2,1)S(1)} %bitcast.55, bf16[2048,2688]{1,0:T(8,128)(2,1)} %all-gather.2.cloned.1.call-done, f32[640]{0:T(1024)S(1)} %copy-done.6), kind=kOutput, calls=%fused_computation.22 | convolution fusion | flops 839065600 | bytes 4753920 | tf_op jit(solution)/shard_map/dot_general | solution.py:83
  308.9 5.4 %convolution_convert_fusion = bf16[320,2048]{1,0:T(8,128)(2,1)S(1)} fusion(bf16[2048,2688]{1,0:T(8,128)(2,1)} %all-gather.2.cloned.1.call-done, bf16[320,2048]{1,0:T(8,128)(2,1)S(1)} %bitcast.56, f32[320,640]{1,0:T(8,128)} %fusion.16, f32[640]{0:T(1024)S(1)} %copy-done.7), kind=kOutput, calls=%fused_computation.2 | convolution fusion | flops 1679810560 | bytes 8686080 | tf_op jit(solution)/shard_map/dot_general | solution.py:102
  314.3 21.2 %all_to_all.44 = bf16[8,40,2048]{2,1,0:T(8,128)(2,1)S(1)} all-to-all(bf16[8,40,2048]{2,1,0:T(8,128)(2,1)S(1)} %bitcast.57), channel_id=1, replica_groups=mesh['rep'=2,'fs'=32,'tp'=8] {'tp'}, dimensions={0} | all-to-all | bytes 2621440 | tf_op jit(solution)/shard_map/all_to_all | solution.py:24
  335.9 21.2 %all_to_all.45 = bf16[8,40,2048]{2,1,0:T(8,128)(2,1)S(1)} all-to-all(bf16[8,40,2048]{2,1,0:T(8,128)(2,1)S(1)} %broadcast_in_dim.11), channel_id=1, replica_groups=mesh['rep'=2,'fs'=32,'tp'=8] {'tp'}, dimensions={0} | all-to-all | bytes 2621440 | tf_op jit(solution)/shard_map/all_to_all | solution.py:54
  357.1 1.1 copy.33
  (49 shorter events, 2.5 us)
Async XLA Ops:
  6.5 166.0 %copy-start = (bf16[320,2048]{1,0:T(8,128)(2,1)S(1)}, bf16[320,2048]{1,0:T(8,128)(2,1)}, u32[]{:S(2)}) copy-start(bf16[320,2048]{1,0:T(8,128)(2,1)} %param.18) | copy-start | bytes 3932164
  6.5 166.0 %copy-start.5 = (f32[2048]{0:T(1024)S(1)}, f32[2048]{0:T(1024)}, u32[]{:S(2)}) copy-start(f32[2048]{0:T(1024)} %param.33) | copy-start | bytes 24580
  6.5 166.0 %copy-start.6 = (f32[640]{0:T(1024)S(1)}, f32[640]{0:T(1024)}, u32[]{:S(2)}) copy-start(f32[640]{0:T(1024)} %param.25) | copy-start | bytes 7684
  6.5 165.9 %all-gather.2.cloned.1.call-start = ((), (), s32[]{:S(2)}) async-start(), calls=%async_computation.8 | async-start | bytes 11354112 | tf_op jit(solution)/shard_map/all_gather | solution.py:31
  12.0 0.7 copy-start.1
  14.1 167.6 %all-to-all-start = ((f32[32,1,128]{2,1,0:T(1,128)}), f32[32,1,128]{2,1,0:T(1,128)S(1)}, u32[]{:S(2)}, u32[]{:S(2)}) async-start(f32[32,1,128]{2,1,0:T(1,128)} %reshape.94), calls=%async_computation | async-start | bytes 32768 | tf_op jit(solution)/shard_map/all_to_all | solution.py:13
  29.3 146.2 %copy-start.7 = (f32[640]{0:T(1024)S(1)}, f32[640]{0:T(1024)}, u32[]{:S(2)}) copy-start(f32[640]{0:T(1024)} %param.26) | copy-start | bytes 7684
  181.8 42.0 %copy-start.3 = (f32[2048]{0:T(1024)S(1)}, f32[2048]{0:T(1024)}, u32[]{:S(2)}) copy-start(f32[2048]{0:T(1024)} %param.34) | copy-start | bytes 24580
  181.8 41.6 %all-to-all-start.1 = ((bf16[8,40,2048]{2,1,0:T(8,128)(2,1)}), bf16[8,40,2048]{2,1,0:T(8,128)(2,1)S(1)}, u32[]{:S(2)}, u32[]{:S(2)}) async-start(bf16[8,40,2048]{2,1,0:T(8,128)(2,1)} %bitcast.51), calls=%async_computation.1 | async-start | bytes 2621440 | tf_op jit(solution)/shard_map/all_to_all | solution.py:24
  223.6 6.0 %copy-start.2 = (f32[31,256]{1,0:T(8,128)S(1)}, f32[31,256]{1,0:T(8,128)}, u32[]{:S(2)}) copy-start(f32[31,256]{1,0:T(8,128)} %param.31) | copy-start | bytes 95236
  223.6 23.8 %copy-start.8 = (f32[256]{0:T(256)S(1)}, f32[256]{0:T(256)}, u32[]{:S(2)}) copy-start(f32[256]{0:T(256)} %param.29) | copy-start | bytes 3076
  225.1 22.3 %all-to-all-start.2 = ((bf16[8,40,2048]{2,1,0:T(8,128)(2,1)}), bf16[8,40,2048]{2,1,0:T(8,128)(2,1)S(1)}, u32[]{:S(2)}, u32[]{:S(2)}) async-start(bf16[8,40,2048]{2,1,0:T(8,128)(2,1)} %broadcast_in_dim.8), calls=%async_computation.2 | async-start | bytes 2621440 | tf_op jit(solution)/shard_map/all_to_all | solution.py:54
  247.4 1.8 copy-start.9
  249.2 11.3 %copy-start.10 = (f32[256]{0:T(256)S(1)}, f32[256]{0:T(256)}, u32[]{:S(2)}) copy-start(f32[256]{0:T(256)} %param.32) | copy-start | bytes 3076
  262.3 21.3 %copy-start.4 = (f32[2048]{0:T(1024)S(1)}, f32[2048]{0:T(1024)}, u32[]{:S(2)}) copy-start(f32[2048]{0:T(1024)} %param.35) | copy-start | bytes 24580
Sparse Core Ops, SparseCore 0:
  12.9 159.5 all-gather.1
